TPU v7x, 32 devices: a whole 2x2x4 slice. The times are simulated.
32 devices in a mesh: sp: 16 (over z, y, x), tp: 2 (over core).
Axes of the slice: x: 2, y: 2, z: 4, core: 2. Of those that a mesh axis runs over, the one named last changes fastest.
Arguments:
- resid: bfloat16 [3072, 2048], P('sp'), may hold values from -6 to 6
- queries: bfloat16 [3072, 1024], P('sp', 'tp'), may hold values from -6.5 to 6.5
- keys: bfloat16 [3072, 1024], P('sp', 'tp'), may hold values from -6.5 to 6.5
- values: bfloat16 [3072, 1024], P('sp', 'tp'), may hold values from -6 to 6
- lambdas: float32 [8], P('tp'), may hold values from 0.3 to 0.8
- head_gain: float32 [128], replicated, may hold values from 0.1 to 1.9
- out_weight: bfloat16 [1024, 2048], P('tp'), may hold values from -0.1875 to 0.1875
- norm_gain: float32 [2048], replicated, may hold values from 0.1 to 1.9
- gate_weight: bfloat16 [2048, 5632], P('sp', 'tp'), may hold values from -0.125 to 0.125
- up_weight: bfloat16 [2048, 5632], P('sp', 'tp'), may hold values from -0.125 to 0.125
- down_weight: bfloat16 [5632, 2048], P('tp', 'sp'), may hold values from -0.078125 to 0.078125
Outputs:
- result: bfloat16 [3072, 2048], P('sp')
All inputs are finite; a program needn't handle non-finite values.
Results may differ from a plain program's by a relative error of at most 0.014.
Values may be sent and summed in bfloat16 or wider, within the bound.
No kernel may reach another device: no remote copies, remote signals or barrier semaphores. Data moves between devices by JAX's collectives and lax.ppermute only.
A program may use at most 128 MiB of HBM per device.

v0:
```python
import jax
import jax.numpy as jnp
from jax import lax
from jax.sharding import PartitionSpec as P

QK = 64
VD = 128


def rms_rows(first, norm_gain):
    return (
        first * lax.rsqrt(jnp.mean(first * first, axis=-1, keepdims=True) + 1e-06) * norm_gain
    ).astype(jnp.bfloat16)


def local(
    resid,
    queries,
    keys,
    values,
    lambdas,
    head_gain,
    out_weight,
    norm_gain,
    gate_weight,
    up_weight,
    down_weight,
):
    tok_rows = queries.shape[0]
    local_heads = lambdas.shape[0]
    model_width = resid.shape[1]
    offset = lax.axis_index("sp") * tok_rows
    query_four = queries.reshape(tok_rows, local_heads, 2, QK)
    score_scale = QK ** (-0.5)
    query_pos = offset + lax.iota(jnp.int32, tok_rows)
    last_query = offset + tok_rows - 1

    def update(fold_state, key_part, value_part, key_pos):
        run_max, run_sum, run_acc = fold_state
        scores = (
            jnp.einsum("qhcd,khcd->chqk", query_four, key_part, preferred_element_type=jnp.float32)
            * score_scale
        )
        causal_mask = key_pos[None, :] <= query_pos[:, None]
        scores = jnp.where(causal_mask, scores, -1e30)
        new_max = jnp.maximum(run_max, jnp.max(scores, axis=-1))
        expo = jnp.where(causal_mask, jnp.exp(scores - new_max[..., None]), 0.0)
        factor = jnp.exp(run_max - new_max)
        new_sum = run_sum * factor + jnp.sum(expo, axis=-1)
        new_acc = run_acc * factor[..., None] + jnp.einsum(
            "chqk,khd->chqd",
            expo.astype(jnp.bfloat16),
            value_part,
            preferred_element_type=jnp.float32,
        )
        return (new_max, new_sum, new_acc)

    initial = (
        jnp.full((2, local_heads, tok_rows), -1e30, jnp.float32),
        jnp.zeros((2, local_heads, tok_rows), jnp.float32),
        jnp.zeros((2, local_heads, tok_rows, VD), jnp.float32),
    )
    key_rows = lax.all_gather(keys, "sp", axis=0, tiled=True)
    value_rows = lax.all_gather(values, "sp", axis=0, tiled=True)
    key_count = key_rows.shape[0]
    key_span = key_count
    while key_span > 1024 and key_span % 2 == 0:
        key_span = key_span // 2

    def one_span(span_index, inner_state):
        span_start = span_index * key_span
        key_part = lax.dynamic_slice_in_dim(key_rows, span_start, key_span, 0).reshape(
            key_span, local_heads, 2, QK
        )
        value_part = lax.dynamic_slice_in_dim(value_rows, span_start, key_span, 0).reshape(
            key_span, local_heads, VD
        )
        key_pos = span_start + lax.iota(jnp.int32, key_span)
        return update(inner_state, key_part, value_part, key_pos)

    def run_spans(inner_state):
        return lax.fori_loop(0, key_count // key_span, one_span, inner_state)

    def keep_state(inner_state):
        return inner_state

    final_max, final_sum, final_acc = lax.cond(
        jnp.int32(0) <= last_query, run_spans, keep_state, initial
    )
    ratio = final_acc / final_sum[..., None]
    mixed_heads = ratio[0] - lambdas[:, None, None] * ratio[1]
    head_out = (
        mixed_heads
        * lax.rsqrt(jnp.mean(mixed_heads * mixed_heads, axis=-1, keepdims=True) + 1e-05)
        * head_gain
    ).astype(jnp.bfloat16)
    out_three = out_weight.reshape(local_heads, VD, model_width)
    own_count = tok_rows // lax.axis_size("tp")
    branch = lax.psum_scatter(
        jnp.einsum("hqd,hde->qe", head_out, out_three, preferred_element_type=jnp.float32).astype(
            jnp.bfloat16
        ),
        "tp",
        scatter_dimension=0,
        tiled=True,
    ).astype(jnp.float32)
    resid_own = lax.dynamic_slice_in_dim(resid, lax.axis_index("tp") * own_count, own_count, 0)
    first = resid_own.astype(jnp.float32) + branch
    normed_all = lax.all_gather(rms_rows(first, norm_gain), "tp", axis=0, tiled=True)
    gate_act = jnp.dot(
        normed_all,
        lax.all_gather(gate_weight, "sp", axis=0, tiled=True),
        preferred_element_type=jnp.float32,
    )
    up_act = jnp.dot(
        normed_all,
        lax.all_gather(up_weight, "sp", axis=0, tiled=True),
        preferred_element_type=jnp.float32,
    )
    hidden = (jax.nn.silu(gate_act) * up_act).astype(jnp.bfloat16)
    terms = jnp.dot(
        hidden,
        lax.all_gather(down_weight, "sp", axis=1, tiled=True),
        preferred_element_type=jnp.float32,
    )
    mixer = lax.psum_scatter(
        terms.astype(jnp.bfloat16), "tp", scatter_dimension=0, tiled=True
    ).astype(jnp.float32)
    finished = (first + 0.5 * mixer).astype(jnp.bfloat16)
    return lax.all_gather(finished, "tp", axis=0, tiled=True)


def solution(mesh):
    return jax.shard_map(
        local,
        mesh=mesh,
        in_specs=(
            P("sp", None),
            P("sp", "tp"),
            P("sp", "tp"),
            P("sp", "tp"),
            P("tp"),
            P(),
            P("tp", None),
            P(),
            P("sp", "tp"),
            P("sp", "tp"),
            P("tp", "sp"),
        ),
        out_specs=P("sp", None),
        check_vma=False,
    )
```

profile of v0, /device:TPU:0, one launch (start us, length us, event | category | flops | bytes accessed | tf_op | source)
XLA Modules:
  0.0 741.6 jit_solution(319168003058939454)
XLA Ops:
  8.1 72.7 %all-gather.6.cloned.1.call-done = bf16[3072,512]{1,0:T(8,128)(2,1)} async-done(((bf16[192,512]{1,0:T(8,128)(2,1)}), bf16[3072,512]{1,0:T(8,128)(2,1)}) %all-gather.6.cloned.1.call-update) | async-done | bytes 3145744 | tf_op jit(solution)/shard_map/all_gather | solution.py:63
  80.7 69.2 %all-gather.8.cloned.1.call-done = bf16[3072,512]{1,0:T(8,128)(2,1)} async-done(((bf16[192,512]{1,0:T(8,128)(2,1)}), bf16[3072,512]{1,0:T(8,128)(2,1)}) %all-gather.8.cloned.1.call-update) | async-done | bytes 3145744 | tf_op jit(solution)/shard_map/all_gather | solution.py:64
  150.0 78.7 %conditional.1 = (f32[2,4,192]{2,1,0:T(4,128)}, f32[2,4,192,128]{3,2,0,1:T(8,128)}) conditional(s32[]{:T(128)} %convert_element_type.38, () %tuple.27, (bf16[192,512]{1,0:T(8,128)(2,1)}, s32[]{:T(128)}, s32[192]{0:T(256)S(1)}, bf16[3072,512]{1,0:T(8,128)(2,1)}, bf16[3072,512]{1,0:T(8,128)(2,1)}) %tuple.28), branch_computations={%region_0.0_spmd, %region_1.6_spmd} | conditional | flops 464347584 | bytes 25131568 | solution.py:87
  151.1 77.6 %while.17 = (s32[]{:T(128)}, f32[2,4,192]{2,1,0:T(4,128)S(1)}, f32[2,4,192]{2,1,0:T(4,128)}, f32[2,4,192,128]{3,2,0,1:T(8,128)}, s32[192]{0:T(256)S(1)}, /*index...) while((s32[]{:T(128)}, f32[2,4,192]{2,1,0:T(4,128)S(1)}, ...), condition=%wide.region_5.5_spmd.clone, body=%wide.region_2.4_spmd.clone.sunk | while | flops 464347392 | bytes 24343476 | solution.py:82
  151.1 2.4 constant_dynamic-slice_fusion.3
  153.5 2.3 copy.60
  155.9 4.2 fusion.41
  160.2 4.3 fusion.42
  166.3 3.6 fusion.44
  169.9 2.4 constant_dynamic-slice_fusion.3
  172.2 2.3 copy.60
  174.7 4.2 fusion.41
  178.9 4.3 fusion.42
  185.7 3.7 fusion.44
  189.5 2.4 constant_dynamic-slice_fusion.3
  191.8 2.3 copy.60
  194.3 4.2 fusion.41
  198.5 4.3 fusion.42
  205.3 3.7 fusion.44
  209.1 2.4 constant_dynamic-slice_fusion.3
  213.9 4.2 fusion.41
  218.1 4.3 fusion.42
  224.9 3.7 fusion.44
  234.5 5.1 reduce-scatter.3.cloned.1.call-done
  242.0 2.5 all_gather.23
  244.5 140.3 %all-gather.10.cloned.1.call-done = bf16[2048,2816]{1,0:T(8,128)(2,1)} async-done(((bf16[128,2816]{1,0:T(8,128)(2,1)}), bf16[2048,2816]{1,0:T(8,128)(2,1)}) %all-gather.10.cloned.1.call-update) | async-done | bytes 11534352 | tf_op jit(solution)/shard_map/all_gather | solution.py:112
  384.7 8.3 %fusion.22 = f32[192,2816]{1,0:T(8,128)} fusion(bf16[192,2048]{1,0:T(8,128)(2,1)} %all_gather.23, bf16[2048,2816]{1,0:T(8,128)(2,1)} %all-gather.10.cloned.1.call-done), kind=kOutput, calls=%fused_computation.42 | convolution fusion | flops 2214592512 | bytes 14483456 | tf_op jit(solution)/shard_map/dot_general | solution.py:110
  393.1 133.9 %all-gather.12.cloned.1.call-done = bf16[2048,2816]{1,0:T(8,128)(2,1)} async-done(((bf16[128,2816]{1,0:T(8,128)(2,1)}), bf16[2048,2816]{1,0:T(8,128)(2,1)}) %all-gather.12.cloned.1.call-update) | async-done | bytes 11534352 | tf_op jit(solution)/shard_map/all_gather | solution.py:117
  527.0 182.8 %all-gather.14.cloned.1.call-done = bf16[2816,2048]{1,0:T(8,128)(2,1)} async-done(((bf16[2816,128]{1,0:T(8,128)(2,1)}), bf16[2816,2048]{1,0:T(8,128)(2,1)}) %all-gather.14.cloned.1.call-update) | async-done | bytes 11534352 | tf_op jit(solution)/shard_map/all_gather | solution.py:123
  709.8 14.0 %convolution_convert_fusion = bf16[192,2048]{1,0:T(8,128)(2,1)} fusion(bf16[2816,2048]{1,0:T(8,128)(2,1)} %all-gather.14.cloned.1.call-done, bf16[192,2048]{1,0:T(8,128)(2,1)} %all_gather.23, bf16[2048,2816]{1,0:T(8,128)(2,1)} %all-gather.12.cloned.1.call-done, f32[192,2816]{1,0:T(8,128)} %fusion.22), kind=kOutput, calls=%fused_computation.25 | convolution fusion | flops 4432822272 | bytes 26804224 | tf_op jit(solution)/shard_map/dot_general | solution.py:121
  723.8 6.5 reduce-scatter.5.cloned.1.call-done
  731.5 2.4 all_gather.27
  (72 shorter events, 24.9 us)
Async XLA Ops:
  6.5 224.6 %copy-start = (bf16[512,2048]{1,0:T(8,128)(2,1)S(1)}, bf16[512,2048]{1,0:T(8,128)(2,1)}, u32[]{:S(2)}) copy-start(bf16[512,2048]{1,0:T(8,128)(2,1)} %param.21) | copy-start | bytes 6291460
  6.5 74.2 %all-gather.6.cloned.1.call-start = ((), (), s32[]{:S(2)}) async-start(), calls=%async_computation.2 | async-start | bytes 3342336 | tf_op jit(solution)/shard_map/all_gather | solution.py:63
  7.3 142.7 %all-gather.8.cloned.1.call-start = ((), (), s32[]{:S(2)}) async-start(), calls=%async_computation.3 | async-start | bytes 3342336 | tf_op jit(solution)/shard_map/all_gather | solution.py:64
  8.0 231.6 %reduce-scatter.3.cloned.1.call-start = ((), (), s32[]{:S(2)}) async-start(), calls=%async_computation.4 | async-start | bytes 1179648 | tf_op jit(solution)/shard_map/reduce_scatter | solution.py:99
  149.9 80.8 %copy-start.4 = (f32[4]{0:T(128)S(1)}, f32[4]{0:T(128)}, u32[]{:S(2)}) copy-start(f32[4]{0:T(128)} %param.19) | copy-start | bytes 52
  149.9 81.2 %copy-start.5 = (f32[128]{0:T(128)S(1)}, f32[128]{0:T(128)}, u32[]{:S(2)}) copy-start(f32[128]{0:T(128)} %param.20) | copy-start | bytes 1540
  231.1 8.5 %copy-start.2 = (bf16[192,2048]{1,0:T(8,128)(2,1)S(1)}, bf16[192,2048]{1,0:T(8,128)(2,1)}, u32[]{:S(2)}) copy-start(bf16[192,2048]{1,0:T(8,128)(2,1)} %param.15) | copy-start | bytes 2359300
  231.1 9.7 %copy-start.3 = (f32[2048]{0:T(1024)S(1)}, f32[2048]{0:T(1024)}, u32[]{:S(2)}) copy-start(f32[2048]{0:T(1024)} %param.22) | copy-start | bytes 24580
  232.7 152.0 %all-gather.10.cloned.1.call-start = ((), (), s32[]{:S(2)}) async-start(), calls=%async_computation.5 | async-start | bytes 12255232 | tf_op jit(solution)/shard_map/all_gather | solution.py:112
  233.3 293.7 %all-gather.12.cloned.1.call-start = ((), (), s32[]{:S(2)}) async-start(), calls=%async_computation.6 | async-start | bytes 12255232 | tf_op jit(solution)/shard_map/all_gather | solution.py:117
  233.9 475.9 %all-gather.14.cloned.1.call-start = ((), (), s32[]{:S(2)}) async-start(), calls=%async_computation.7 | async-start | bytes 12255232 | tf_op jit(solution)/shard_map/all_gather | solution.py:123
  234.4 495.9 %reduce-scatter.5.cloned.1.call-start = ((), (), s32[]{:S(2)}) async-start(), calls=%async_computation.8 | async-start | bytes 1179648 | tf_op jit(solution)/shard_map/reduce_scatter | solution.py:126
  393.1 337.3 %copy-start.1 = (bf16[96,2048]{1,0:T(8,128)(2,1)S(1)}, bf16[96,2048]{1,0:T(8,128)(2,1)}, u32[]{:S(2)}) copy-start(bf16[96,2048]{1,0:T(8,128)(2,1)} %reduce-scatter.3.cloned.1.call-done) | copy-start | bytes 1179652
Sparse Core Ops, SparseCore 0:
  10.1 70.5 all-gather.5
  83.5 66.3 all-gather.7
  232.8 6.6 reduce-scatter.2
  242.2 142.5 all-gather.9
  387.3 139.5 all-gather.11
  529.5 180.2 all-gather.13
  723.9 6.3 reduce-scatter.4
where the time goes:
time: 743 us; the launch traced here: 742 us
  waiting for transfers between devices  613 us (83%)
  matrix products  55.5 us (7%)
  other arithmetic  27.8 us (4%)
  local copies, waits for them, and re-layouts  26 us (3%)
  between operations  13.6 us (2%)
    all_gather x1, waiting for transfers between devices, local(): lax.all_gather(down_weight, 'sp', axis=1, tiled=True)  183 us
    all_gather x1, waiting for transfers between devices, local(): lax.all_gather(gate_weight, 'sp', axis=0, tiled=True)  140 us
    all_gather x1, waiting for transfers between devices, local(): lax.all_gather(up_weight, 'sp', axis=0, tiled=True)  134 us
    all_gather x1, waiting for transfers between devices, local(): key_rows = lax.all_gather(keys, 'sp', axis=0, tiled=True)  72.7 us
    all_gather x1, waiting for transfers between devices, local(): value_rows = lax.all_gather(values, 'sp', axis=0, tiled=True)  69.2 us
    convert_element_type x4, other arithmetic, update(): expo.astype(jnp.bfloat16)  17.4 us
    dot_general x4, matrix products, update(): jnp.einsum('qhcd,khcd->chqk', query_four, key_part, preferred_element_typ...  16.9 us
  transfers between devices with their start and end apart: 7, of which 7 were waited for; matrix products, arithmetic and copies ran while one was open for 1% of the time, Pallas kernels for 0%

commit v1 on v0

--- a/solution.py
+++ b/solution.py
@@ -120,7 +120,7 @@
     hidden = (jax.nn.silu(gate_act) * up_act).astype(jnp.bfloat16)
     terms = jnp.dot(
         hidden,
-        lax.all_gather(down_weight, "sp", axis=1, tiled=True),
+        jnp.concatenate(lax.all_gather(down_weight, "sp"), axis=1),
         preferred_element_type=jnp.float32,
     )
     mixer = lax.psum_scatter(

time: 743 us -> 704 us (0.948)
  waiting for transfers between devices: 613 us -> 558 us
  local copies, waits for them, and re-layouts: 26 us -> 41.1 us
    all_gather x1, waiting for transfers between devices: 183 us -> 140 us  [local(): lax.all_gather(down_weight, 'sp')]
    reshape x0 -> x1, local copies, waits for them, and re-layouts: none -> 15.2 us  [local(): jnp.concatenate(lax.all_gather(down_weight, 'sp'), axis=1)]
    all_gather x1, waiting for transfers between devices: 140 us -> 127 us  [local(): lax.all_gather(gate_weight, 'sp', axis=0, tiled=True)]
  transfers between devices with their start and end apart: 7 -> 7, of which waited for: 7 -> 7; matrix products, arithmetic and copies ran while one was open for 1% -> 4% of each run, Pallas kernels for 0% -> 0%
where the time goes in v1:
time: 704 us; the launch traced here: 703 us
  waiting for transfers between devices  558 us (79%)
  matrix products  56.8 us (8%)
  local copies, waits for them, and re-layouts  41.1 us (6%)
  other arithmetic  27.9 us (4%)
  between operations  13.6 us (2%)
    all_gather x1, waiting for transfers between devices, local(): lax.all_gather(down_weight, 'sp')  140 us
    all_gather x1, waiting for transfers between devices, local(): lax.all_gather(up_weight, 'sp', axis=0, tiled=True)  134 us
    all_gather x1, waiting for transfers between devices, local(): lax.all_gather(gate_weight, 'sp', axis=0, tiled=True)  127 us
    all_gather x1, waiting for transfers between devices, local(): key_rows = lax.all_gather(keys, 'sp', axis=0, tiled=True)  72.7 us
    all_gather x1, waiting for transfers between devices, local(): value_rows = lax.all_gather(values, 'sp', axis=0, tiled=True)  69.2 us
    convert_element_type x4, other arithmetic, update(): expo.astype(jnp.bfloat16)  17.4 us
    dot_general x4, matrix products, update(): jnp.einsum('qhcd,khcd->chqk', query_four, key_part, preferred_element_typ...  16.8 us
    dot_general x1, matrix products, local(): jnp.dot(hidden, jnp.concatenate(lax.all_gather(down_weight, 'sp'), axis=1...  15.6 us
  transfers between devices with their start and end apart: 7, of which 7 were waited for; matrix products, arithmetic and copies ran while one was open for 4% of the time, Pallas kernels for 0%

profile of v1, /device:TPU:0, one launch (start us, length us, event | category | flops | bytes accessed | tf_op | source)
XLA Modules:
  0.0 702.6 jit_solution(13149514545786928006)
XLA Ops:
  8.1 72.7 %all-gather.7.cloned.1.call-done = bf16[3072,512]{1,0:T(8,128)(2,1)} async-done(((bf16[192,512]{1,0:T(8,128)(2,1)}), bf16[3072,512]{1,0:T(8,128)(2,1)}) %all-gather.7.cloned.1.call-update) | async-done | bytes 3145744 | tf_op jit(solution)/shard_map/all_gather | solution.py:63
  80.7 69.2 %all-gather.9.cloned.1.call-done = bf16[3072,512]{1,0:T(8,128)(2,1)} async-done(((bf16[192,512]{1,0:T(8,128)(2,1)}), bf16[3072,512]{1,0:T(8,128)(2,1)}) %all-gather.9.cloned.1.call-update) | async-done | bytes 3145744 | tf_op jit(solution)/shard_map/all_gather | solution.py:64
  150.0 78.7 %conditional.1 = (f32[2,4,192]{2,1,0:T(4,128)}, f32[2,4,192,128]{3,2,0,1:T(8,128)}) conditional(s32[]{:T(128)} %convert_element_type.38, () %tuple.27, (bf16[192,512]{1,0:T(8,128)(2,1)}, s32[]{:T(128)}, s32[192]{0:T(256)S(1)}, bf16[3072,512]{1,0:T(8,128)(2,1)}, bf16[3072,512]{1,0:T(8,128)(2,1)}) %tuple.28), branch_computations={%region_0.0_spmd, %region_1.6_spmd} | conditional | flops 464347584 | bytes 25131568 | solution.py:87
  151.1 77.6 %while.17 = (s32[]{:T(128)}, f32[2,4,192]{2,1,0:T(4,128)S(1)}, f32[2,4,192]{2,1,0:T(4,128)}, f32[2,4,192,128]{3,2,0,1:T(8,128)}, s32[192]{0:T(256)S(1)}, /*index...) while((s32[]{:T(128)}, f32[2,4,192]{2,1,0:T(4,128)S(1)}, ...), condition=%wide.region_5.5_spmd.clone, body=%wide.region_2.4_spmd.clone.sunk | while | flops 464347392 | bytes 24343476 | solution.py:82
  151.1 2.4 constant_dynamic-slice_fusion.3
  153.5 2.3 copy.72
  155.9 4.2 fusion.41
  160.1 4.3 fusion.42
  166.3 3.6 fusion.44
  169.9 2.4 constant_dynamic-slice_fusion.3
  172.2 2.3 copy.72
  174.7 4.2 fusion.41
  178.9 4.3 fusion.42
  185.7 3.7 fusion.44
  189.4 2.4 constant_dynamic-slice_fusion.3
  194.3 4.2 fusion.41
  198.5 4.3 fusion.42
  205.3 3.7 fusion.44
  209.0 2.4 constant_dynamic-slice_fusion.3
  213.8 4.2 fusion.41
  218.1 4.3 fusion.42
  224.9 3.7 fusion.44
  234.5 5.1 reduce-scatter.3.cloned.1.call-done
  241.9 2.5 all_gather.26
  244.5 140.2 %all-gather.15.cloned.1.call-done = bf16[45056,128]{1,0:T(8,128)(2,1)} async-done(((bf16[2816,128]{1,0:T(8,128)(2,1)}), bf16[45056,128]{1,0:T(8,128)(2,1)}) %all-gather.15.cloned.1.call-update) | async-done | bytes 11534352 | tf_op jit(solution)/shard_map/all_gather | solution.py:123
  384.7 15.2 %copy.48 = bf16[2816,16,128]{0,2,1:T(8,128)(2,1)} copy(bf16[2816,16,128]{2,0,1:T(8,128)(2,1)} %bitcast.77) | data formatting | bytes 23068672 | tf_op jit(solution)/shard_map/reshape | solution.py:123
  399.9 127.0 %all-gather.11.cloned.1.call-done = bf16[2048,2816]{1,0:T(8,128)(2,1)} async-done(((bf16[128,2816]{1,0:T(8,128)(2,1)}), bf16[2048,2816]{1,0:T(8,128)(2,1)}) %all-gather.11.cloned.1.call-update) | async-done | bytes 11534352 | tf_op jit(solution)/shard_map/all_gather | solution.py:112
  526.9 8.0 %fusion.22 = f32[192,2816]{1,0:T(8,128)} fusion(bf16[192,2048]{1,0:T(8,128)(2,1)S(1)} %all_gather.26, bf16[2048,2816]{1,0:T(8,128)(2,1)} %all-gather.11.cloned.1.call-done), kind=kOutput, calls=%fused_computation.42 | convolution fusion | flops 2214592512 | bytes 14483456 | tf_op jit(solution)/shard_map/dot_general | solution.py:110
  535.0 134.2 %all-gather.13.cloned.1.call-done = bf16[2048,2816]{1,0:T(8,128)(2,1)} async-done(((bf16[128,2816]{1,0:T(8,128)(2,1)}), bf16[2048,2816]{1,0:T(8,128)(2,1)}) %all-gather.13.cloned.1.call-update) | async-done | bytes 11534352 | tf_op jit(solution)/shard_map/all_gather | solution.py:117
  669.2 15.6 %convolution_convert_fusion = bf16[192,2048]{1,0:T(8,128)(2,1)} fusion(bf16[2816,2048]{0,1:T(8,128)(2,1)} %bitcast.78, bf16[192,2048]{1,0:T(8,128)(2,1)} %copy-done.4, bf16[2048,2816]{1,0:T(8,128)(2,1)} %all-gather.13.cloned.1.call-done, f32[192,2816]{1,0:T(8,128)} %fusion.22), kind=kOutput, calls=%fused_computation.25 | convolution fusion | flops 4432822272 | bytes 26804224 | tf_op jit(solution)/shard_map/dot_general | solution.py:121
  684.8 6.5 reduce-scatter.5.cloned.1.call-done
  692.5 2.4 all_gather.31
  (77 shorter events, 27.2 us)
Async XLA Ops:
  6.5 224.5 %copy-start = (bf16[512,2048]{1,0:T(8,128)(2,1)S(1)}, bf16[512,2048]{1,0:T(8,128)(2,1)}, u32[]{:S(2)}) copy-start(bf16[512,2048]{1,0:T(8,128)(2,1)} %param.21) | copy-start | bytes 6291460
  6.5 74.2 %all-gather.7.cloned.1.call-start = ((), (), s32[]{:S(2)}) async-start(), calls=%async_computation.2 | async-start | bytes 3342336 | tf_op jit(solution)/shard_map/all_gather | solution.py:63
  7.3 142.7 %all-gather.9.cloned.1.call-start = ((), (), s32[]{:S(2)}) async-start(), calls=%async_computation.3 | async-start | bytes 3342336 | tf_op jit(solution)/shard_map/all_gather | solution.py:64
  8.0 231.5 %reduce-scatter.3.cloned.1.call-start = ((), (), s32[]{:S(2)}) async-start(), calls=%async_computation.4 | async-start | bytes 1179648 | tf_op jit(solution)/shard_map/reduce_scatter | solution.py:99
  149.9 80.8 %copy-start.6 = (f32[4]{0:T(128)S(1)}, f32[4]{0:T(128)}, u32[]{:S(2)}) copy-start(f32[4]{0:T(128)} %param.19) | copy-start | bytes 52
  149.9 81.1 %copy-start.7 = (f32[128]{0:T(128)S(1)}, f32[128]{0:T(128)}, u32[]{:S(2)}) copy-start(f32[128]{0:T(128)} %param.20) | copy-start | bytes 1540
  231.1 8.5 %copy-start.3 = (bf16[192,2048]{1,0:T(8,128)(2,1)S(1)}, bf16[192,2048]{1,0:T(8,128)(2,1)}, u32[]{:S(2)}) copy-start(bf16[192,2048]{1,0:T(8,128)(2,1)} %param.15) | copy-start | bytes 2359300
  231.1 9.7 %copy-start.5 = (f32[2048]{0:T(1024)S(1)}, f32[2048]{0:T(1024)}, u32[]{:S(2)}) copy-start(f32[2048]{0:T(1024)} %param.22) | copy-start | bytes 24580
  232.7 152.0 %all-gather.15.cloned.1.call-start = ((), (), s32[]{:S(2)}) async-start(), calls=%async_computation.8 | async-start | bytes 12255232 | tf_op jit(solution)/shard_map/all_gather | solution.py:123
  233.2 293.7 %all-gather.11.cloned.1.call-start = ((), (), s32[]{:S(2)}) async-start(), calls=%async_computation.5 | async-start | bytes 12255232 | tf_op jit(solution)/shard_map/all_gather | solution.py:112
  233.8 435.4 %all-gather.13.cloned.1.call-start = ((), (), s32[]{:S(2)}) async-start(), calls=%async_computation.6 | async-start | bytes 12255232 | tf_op jit(solution)/shard_map/all_gather | solution.py:117
  234.4 456.9 %reduce-scatter.5.cloned.1.call-start = ((), (), s32[]{:S(2)}) async-start(), calls=%async_computation.7 | async-start | bytes 1179648 | tf_op jit(solution)/shard_map/reduce_scatter | solution.py:126
  244.5 282.5 %copy-start.4 = (bf16[192,2048]{1,0:T(8,128)(2,1)}, bf16[192,2048]{1,0:T(8,128)(2,1)S(1)}, u32[]{:S(2)}) copy-start(bf16[192,2048]{1,0:T(8,128)(2,1)S(1)} %all_gather.26) | copy-start | bytes 2359300
  669.2 22.1 %copy-start.2 = (bf16[96,2048]{1,0:T(8,128)(2,1)S(1)}, bf16[96,2048]{1,0:T(8,128)(2,1)}, u32[]{:S(2)}) copy-start(bf16[96,2048]{1,0:T(8,128)(2,1)} %reduce-scatter.3.cloned.1.call-done) | copy-start | bytes 1179652
  669.2 26.5 %copy-start.1 = (bf16[512,2048]{1,0:T(8,128)(2,1)S(1)}, bf16[512,2048]{1,0:T(8,128)(2,1)}, u32[]{:S(2)}) copy-start(bf16[512,2048]{1,0:T(8,128)(2,1)} %param.21) | copy-start | bytes 6291460
Sparse Core Ops, SparseCore 0:
  10.1 70.5 all-gather.6
  83.5 66.3 all-gather.8
  232.8 6.6 reduce-scatter.2
  242.1 142.5 all-gather.14
  387.3 139.5 all-gather.10
  529.5 139.5 all-gather.12
  684.9 6.3 reduce-scatter.4
